TPU v7x, 32 devices: a whole 2x2x4 slice. The times are simulated.
32 devices in a mesh: sp: 8 (over z, y), tp: 4 (over x, core).
Axes of the slice: x: 2, y: 2, z: 4, core: 2. Of those that a mesh axis runs over, the one named last changes fastest.
Arguments:
- queries: bfloat16 [4096, 1024], P('sp', 'tp'), may hold values from -6 to 6
- key_heads: bfloat16 [4096, 512], P('sp', 'tp'), may hold values from -6 to 6
- value_heads: bfloat16 [4096, 512], P('sp', 'tp'), may hold values from -70 to 70
- documents: int32 [4096], P('sp'), may hold values from 0 to 2, never falling along the last dimension, each value on 1 to 2560 neighbouring positions
- query_gain: float32 [128], replicated, may hold values from 0.1 to 8
- key_gain: float32 [128], replicated, may hold values from 0.1 to 8
- out_gain: float32 [1024], replicated, may hold values from 0.1 to 1.9
- out_proj: bfloat16 [1024, 2048], replicated, may hold values from -0.1875 to 0.1875
- residual: bfloat16 [4096, 2048], P(('sp', 'tp')), may hold values from -6 to 6
- mid_gain: float32 [2048], replicated, may hold values from 0.1 to 1.9
- mid_bias: float32 [2048], replicated, may hold values from -1.5 to 1.5
- routes: int32 [4096, 2], P(('sp', 'tp')), may hold values from 0 to 31, all different within a row; in each aligned block of 128 rows (0 to 127, 128 to 255, ...) at most 16 rows name the same one
- route_weights: float32 [4096, 2], P(('sp', 'tp')), may hold values from 0.2 to 2
- expert_gate: bfloat16 [32, 2048, 512], P(('sp', 'tp')), may hold values from -0.125 to 0.125
- expert_up: bfloat16 [32, 2048, 512], P(('sp', 'tp')), may hold values from -0.125 to 0.125
- expert_down: bfloat16 [32, 512, 2048], P(('sp', 'tp')), may hold values from -0.25 to 0.25
- final_gain: float32 [2048], replicated, may hold values from 0.1 to 1.9
- final_bias: float32 [2048], replicated, may hold values from -1.5 to 1.5
Outputs:
- layer_out: bfloat16 [4096, 2048], P(('sp', 'tp'))
Inputs may be any that keep to these rules, and one draw needn't show every extreme that they name: `documents`: never falls along the sequence; each document holds 1 to 2560 positions and one holds exactly 2560. `routes`: each row names 2 different experts; among the rows of one device (aligned blocks of 128 rows) no expert is named more than 16 times, and exactly 16 times in some block.
All inputs are finite; a program needn't handle non-finite values.
Results may differ from a plain program's by a relative error of at most 0.014.
The roundings to bfloat16 on the way count: a program that leaves them out, or rounds other values in their place, can miss the bound.
Values may be sent and summed in bfloat16 or wider, within the bound.
A program may use at most 128 MiB of HBM per device.

v0:
```python
import math
import jax
import jax.numpy as jnp
from jax import lax
from jax.sharding import PartitionSpec as P

HEAD = 128
GRID = 64
eps_norm = 1e-06
alpha_mix = 8.0**0.25
theta_base = 10000.0


def rotary_tables(row_total, offset):
    positions = offset + jnp.arange(row_total, dtype=jnp.int32)
    grid_row = (positions // GRID).astype(jnp.float32)
    grid_col = (positions % GRID).astype(jnp.float32)
    pair_count = HEAD // 4
    inv_freq = theta_base ** (-jnp.arange(pair_count, dtype=jnp.float32) / pair_count)
    angles = jnp.concatenate(
        [grid_row[:, None] * inv_freq[None, :], grid_col[:, None] * inv_freq[None, :]], axis=1
    )
    return (jnp.cos(angles), jnp.sin(angles))


def normed_rotated(heads_in, gain_vec, cosine_table, sine_table):
    values = heads_in.astype(jnp.float32)
    inv_rms = lax.rsqrt(jnp.mean(values * values, axis=-1, keepdims=True) + eps_norm)
    values = values * inv_rms * gain_vec
    half_dim = HEAD // 2
    first_half = values[..., :half_dim]
    second_half = values[..., half_dim:]
    cosine_part = cosine_table[:, None, :]
    sine_part = sine_table[:, None, :]
    turned = jnp.concatenate(
        [
            first_half * cosine_part - second_half * sine_part,
            second_half * cosine_part + first_half * sine_part,
        ],
        axis=-1,
    )
    return turned.astype(jnp.bfloat16)


def layer_norm(stream, gain_vec, bias_vec):
    center = jnp.mean(stream, axis=-1, keepdims=True)
    spread = jnp.mean(jnp.square(stream - center), axis=-1, keepdims=True)
    return (stream - center) * lax.rsqrt(spread + eps_norm) * gain_vec + bias_vec


def per_device(
    queries,
    key_heads,
    value_heads,
    documents,
    query_gain,
    key_gain,
    out_gain,
    out_proj,
    residual,
    mid_gain,
    mid_bias,
    routes,
    route_weights,
    expert_gate,
    expert_up,
    expert_down,
    final_gain,
    final_bias,
):
    tok_rows = queries.shape[0]
    query_local = queries.shape[1] // HEAD
    key_local = key_heads.shape[1] // HEAD
    grouped = query_local // key_local
    offset = lax.axis_index("sp") * tok_rows
    cosine_table, sine_table = rotary_tables(tok_rows, offset)
    query_rot = normed_rotated(
        queries.reshape(tok_rows, query_local, HEAD), query_gain, cosine_table, sine_table
    ).reshape(tok_rows, key_local, grouped, HEAD)
    key_rot = normed_rotated(
        key_heads.reshape(tok_rows, key_local, HEAD), key_gain, cosine_table, sine_table
    ).reshape(tok_rows, key_local * HEAD)
    first_doc = documents[0]
    last_doc = documents[tok_rows - 1]
    start_state = (
        jnp.full((key_local, grouped, tok_rows), -1e30, jnp.float32),
        jnp.zeros((key_local, grouped, tok_rows), jnp.float32),
        jnp.zeros((key_local, grouped, tok_rows, HEAD), jnp.float32),
    )
    key_part = lax.all_gather(key_rot, "sp", axis=0, tiled=True)
    value_part = lax.all_gather(value_heads, "sp", axis=0, tiled=True)
    doc_part = lax.all_gather(documents, "sp", axis=0, tiled=True)
    piece_rows = key_part.shape[0]
    block_rows = math.gcd(piece_rows, 512)
    block_count = piece_rows // block_rows
    blocks = (
        key_part.reshape(block_count, block_rows, key_local, HEAD),
        value_part.reshape(block_count, block_rows, key_local, HEAD),
        doc_part.reshape(block_count, block_rows),
    )

    def advance(running, block_set):
        key_block, value_block, doc_block = block_set
        running_max, running_total, running_sum = running
        scores = jnp.einsum(
            "qkgd,tkd->kgqt", query_rot, key_block, preferred_element_type=jnp.float32
        ) * HEAD ** (-0.5)
        allowed = (documents[:, None] == doc_block[None, :])[None, None]
        scores = jnp.where(allowed, scores, -1e30)
        new_max = jnp.maximum(running_max, jnp.max(scores, axis=-1))
        weights = jnp.where(allowed, jnp.exp(scores - new_max[..., None]), 0.0)
        rescale = jnp.exp(running_max - new_max)
        new_total = running_total * rescale + jnp.sum(weights, axis=-1)
        new_sum = running_sum * rescale[..., None] + jnp.einsum(
            "kgqt,tkd->kgqd",
            weights.astype(jnp.bfloat16),
            value_block,
            preferred_element_type=jnp.float32,
        )
        return ((new_max, new_total, new_sum), None)

    def process(running):
        result, unused = lax.scan(advance, running, blocks)
        return result

    touches = (doc_part[0] <= last_doc) & (doc_part[piece_rows - 1] >= first_doc)
    final_max, final_total, final_sum = lax.cond(
        touches, process, lambda running: running, start_state
    )
    attention = jnp.transpose(final_sum / final_total[..., None], (2, 0, 1, 3))
    attention = attention.reshape(tok_rows, query_local * HEAD).astype(jnp.bfloat16)
    whole_rows = lax.all_to_all(attention, "tp", split_axis=0, concat_axis=1, tiled=True)
    whole_float = whole_rows.astype(jnp.float32)
    mean_square = jnp.mean(whole_float * whole_float, axis=1)
    scaled = (whole_float * out_gain).astype(jnp.bfloat16)
    projected = jnp.dot(scaled, out_proj, preferred_element_type=jnp.float32)
    projected = projected * lax.rsqrt(mean_square + eps_norm)[:, None]
    middle = layer_norm(
        alpha_mix * residual.astype(jnp.float32) + projected, mid_gain, mid_bias
    ).astype(jnp.bfloat16)
    out_rows = middle.shape[0]
    model_width = middle.shape[1]
    top_count = routes.shape[1]
    local_experts = expert_gate.shape[0]
    sp_size = lax.axis_size("sp")
    tp_size = lax.axis_size("tp")
    expert_total = local_experts * sp_size * tp_size
    capacity = 2 * out_rows * top_count // expert_total
    flat_routes = routes.reshape(-1)
    one_hot = (flat_routes[:, None] == jnp.arange(expert_total, dtype=jnp.int32)[None, :]).astype(
        jnp.int32
    )
    rank_in = jnp.sum((jnp.cumsum(one_hot, axis=0) - one_hot) * one_hot, axis=1)
    target = flat_routes * capacity + rank_in
    outbound = (
        jnp.zeros((expert_total * capacity, model_width), jnp.bfloat16)
        .at[target]
        .set(jnp.repeat(middle, top_count, axis=0))
    )
    arrived = lax.all_to_all(
        outbound.reshape(expert_total, capacity, model_width),
        ("sp", "tp"),
        split_axis=0,
        concat_axis=0,
        tiled=True,
    )
    item_count = arrived.shape[-2]
    grouped_rows = arrived.reshape(-1, local_experts, item_count, model_width)
    gate_part = jnp.einsum(
        "sekd,edf->sekf", grouped_rows, expert_gate, preferred_element_type=jnp.float32
    )
    up_part = jnp.einsum(
        "sekd,edf->sekf", grouped_rows, expert_up, preferred_element_type=jnp.float32
    )
    hidden = (jax.nn.silu(gate_part) * up_part).astype(jnp.bfloat16)
    served = jnp.einsum("sekf,efd->sekd", hidden, expert_down, preferred_element_type=jnp.float32)
    returned = lax.all_to_all(
        served.astype(jnp.bfloat16).reshape(arrived.shape),
        ("sp", "tp"),
        split_axis=0,
        concat_axis=0,
        tiled=True,
    )
    picked = returned.reshape(expert_total * capacity, model_width)[target]
    picked = picked.astype(jnp.float32).reshape(out_rows, top_count, model_width)
    routed = jnp.sum(picked * route_weights[:, :, None], axis=1)
    return layer_norm(
        alpha_mix * middle.astype(jnp.float32) + routed, final_gain, final_bias
    ).astype(jnp.bfloat16)


def solution(mesh):
    return jax.shard_map(
        per_device,
        mesh=mesh,
        in_specs=(
            P("sp", "tp"),
            P("sp", "tp"),
            P("sp", "tp"),
            P("sp"),
            P(),
            P(),
            P(),
            P(),
            P(("sp", "tp"), None),
            P(),
            P(),
            P(("sp", "tp"), None),
            P(("sp", "tp"), None),
            P(("sp", "tp"), None, None),
            P(("sp", "tp"), None, None),
            P(("sp", "tp"), None, None),
            P(),
            P(),
        ),
        out_specs=P(("sp", "tp"), None),
        check_vma=False,
    )
```

profile of v0, /device:TPU:0, one launch (start us, length us, event | category | flops | bytes accessed | tf_op | source)
XLA Modules:
  0.0 323.6 jit_solution(3362261494470061725)
XLA Ops:
  11.2 27.9 %all-gather = s32[8,1,512]{2,1,0:T(1,128)S(1)} all-gather(s32[1,1,512]{2,1,0:T(1,128)S(1)} %bitcast.186), channel_id=1, replica_groups=mesh['sp'=8,'tp'=4] {'sp'}, dimensions={0}, use_global_device_ids=true | all-gather | bytes 18432 | tf_op jit(solution)/shard_map/all_gather | solution.py:92
  44.9 7.3 %all-gather.4.cloned.1.call-done = bf16[4096,128]{0,1:T(8,128)(2,1)} async-done(((bf16[512,128]{0,1:T(8,128)(2,1)}), bf16[4096,128]{0,1:T(8,128)(2,1)}) %all-gather.4.cloned.1.call-update) | async-done | bytes 1048592 | tf_op jit(solution)/shard_map/all_gather | solution.py:90
  52.2 41.4 %all-gather.6.cloned.1.call-done = bf16[4096,128]{1,0:T(8,128)(2,1)} async-done(((bf16[512,128]{1,0:T(8,128)(2,1)}), bf16[4096,128]{1,0:T(8,128)(2,1)}) %all-gather.6.cloned.1.call-update) | async-done | bytes 1048592 | tf_op jit(solution)/shard_map/all_gather | solution.py:91
  93.6 69.2 %conditional.1 = (f32[1,2,512]{2,1,0:T(2,128)}, f32[1,2,512,128]{3,2,1,0:T(8,128)}) conditional(s32[]{:T(128)} %bitcast.4, () %tuple.17, (bf16[4096,128]{0,1:T(8,128)(2,1)}, bf16[4096,128]{1,0:T(8,128)(2,1)}, s32[4096]{0:T(1024)S(1)}, s32[512]{0:T(512)S(1)}, bf16[512,1,2,128]{0,3,2,1:T(8,128)(2,1)S(1)}) %tuple.62), branch_computations={%region_2.3_spmd, %region_3.8_spmd} | conditional | flops 275912704 | bytes 20030728 | solution.py:127
  96.1 66.7 %while.14 = (s32[]{:T(128)}, f32[1,2,512]{2,1,0:T(2,128)S(1)}, f32[1,2,512]{2,1,0:T(2,128)}, f32[1,2,512,128]{3,2,1,0:T(8,128)}, s32[512]{0:T(512)S(1)}, /*index...) while((s32[]{:T(128)}, f32[1,2,512]{2,1,0:T(2,128)S(1)}, ...), condition=%wide.region_7.7_spmd.clone, body=%wide.region_4.6_spmd.clone.sunk | while | flops 275912704 | bytes 17376408 | solution.py:123
  96.4 2.8 fusion.93
  99.2 3.4 %fusion.96 = f32[1,2,512,128]{3,2,1,0:T(8,128)} fusion(f32[512,512,2]{1,0,2:T(8,128)} %get-tuple-element.223, f32[2,512]{1,0:T(2,128)S(1)} %bitcast.183, pred[512,512]{0,1:T(8,128)(4,1)S(1)} %broadcast_compare_fusion.2, f32[1,2,512,128]{3,2,1,0:T(8,128)} %get-tuple-element.239, f32[2,512]{1,0:T(2,128)S(1)} %get-tuple-element.224, pred[]{:T(512)S(6)} %compare.14, ...), kind=kOutput, calls=%fused_computation.8.clone.1 | convolution fusion | flops 137232384 | bytes 3547649 | tf_op jit(solution)/shard_map/cond/branch_1_fun/while/body/eval_jaxpr/kgqt,tkd->kgqd/dot_general | solution.py:114
  104.0 2.8 fusion.93
  106.8 3.5 %fusion.96 = f32[1,2,512,128]{3,2,1,0:T(8,128)} fusion(f32[512,512,2]{1,0,2:T(8,128)} %get-tuple-element.223, f32[2,512]{1,0:T(2,128)S(1)} %bitcast.183, pred[512,512]{0,1:T(8,128)(4,1)S(1)} %broadcast_compare_fusion.2, f32[1,2,512,128]{3,2,1,0:T(8,128)} %get-tuple-element.239, f32[2,512]{1,0:T(2,128)S(1)} %get-tuple-element.224, pred[]{:T(512)S(6)} %compare.14, ...), kind=kOutput, calls=%fused_computation.8.clone.1 | convolution fusion | flops 137232384 | bytes 3547649 | tf_op jit(solution)/shard_map/cond/branch_1_fun/while/body/eval_jaxpr/kgqt,tkd->kgqd/dot_general | solution.py:114
  112.4 2.8 fusion.93
  115.3 3.5 %fusion.96 = f32[1,2,512,128]{3,2,1,0:T(8,128)} fusion(f32[512,512,2]{1,0,2:T(8,128)} %get-tuple-element.223, f32[2,512]{1,0:T(2,128)S(1)} %bitcast.183, pred[512,512]{0,1:T(8,128)(4,1)S(1)} %broadcast_compare_fusion.2, f32[1,2,512,128]{3,2,1,0:T(8,128)} %get-tuple-element.239, f32[2,512]{1,0:T(2,128)S(1)} %get-tuple-element.224, pred[]{:T(512)S(6)} %compare.14, ...), kind=kOutput, calls=%fused_computation.8.clone.1 | convolution fusion | flops 137232384 | bytes 3547649 | tf_op jit(solution)/shard_map/cond/branch_1_fun/while/body/eval_jaxpr/kgqt,tkd->kgqd/dot_general | solution.py:114
  120.9 2.8 fusion.93
  123.7 3.5 %fusion.96 = f32[1,2,512,128]{3,2,1,0:T(8,128)} fusion(f32[512,512,2]{1,0,2:T(8,128)} %get-tuple-element.223, f32[2,512]{1,0:T(2,128)S(1)} %bitcast.183, pred[512,512]{0,1:T(8,128)(4,1)S(1)} %broadcast_compare_fusion.2, f32[1,2,512,128]{3,2,1,0:T(8,128)} %get-tuple-element.239, f32[2,512]{1,0:T(2,128)S(1)} %get-tuple-element.224, pred[]{:T(512)S(6)} %compare.14, ...), kind=kOutput, calls=%fused_computation.8.clone.1 | convolution fusion | flops 137232384 | bytes 3547649 | tf_op jit(solution)/shard_map/cond/branch_1_fun/while/body/eval_jaxpr/kgqt,tkd->kgqd/dot_general | solution.py:114
  129.3 2.8 fusion.93
  132.1 3.5 %fusion.96 = f32[1,2,512,128]{3,2,1,0:T(8,128)} fusion(f32[512,512,2]{1,0,2:T(8,128)} %get-tuple-element.223, f32[2,512]{1,0:T(2,128)S(1)} %bitcast.183, pred[512,512]{0,1:T(8,128)(4,1)S(1)} %broadcast_compare_fusion.2, f32[1,2,512,128]{3,2,1,0:T(8,128)} %get-tuple-element.239, f32[2,512]{1,0:T(2,128)S(1)} %get-tuple-element.224, pred[]{:T(512)S(6)} %compare.14, ...), kind=kOutput, calls=%fused_computation.8.clone.1 | convolution fusion | flops 137232384 | bytes 3547649 | tf_op jit(solution)/shard_map/cond/branch_1_fun/while/body/eval_jaxpr/kgqt,tkd->kgqd/dot_general | solution.py:114
  137.7 2.8 fusion.93
  140.6 3.5 %fusion.96 = f32[1,2,512,128]{3,2,1,0:T(8,128)} fusion(f32[512,512,2]{1,0,2:T(8,128)} %get-tuple-element.223, f32[2,512]{1,0:T(2,128)S(1)} %bitcast.183, pred[512,512]{0,1:T(8,128)(4,1)S(1)} %broadcast_compare_fusion.2, f32[1,2,512,128]{3,2,1,0:T(8,128)} %get-tuple-element.239, f32[2,512]{1,0:T(2,128)S(1)} %get-tuple-element.224, pred[]{:T(512)S(6)} %compare.14, ...), kind=kOutput, calls=%fused_computation.8.clone.1 | convolution fusion | flops 137232384 | bytes 3547649 | tf_op jit(solution)/shard_map/cond/branch_1_fun/while/body/eval_jaxpr/kgqt,tkd->kgqd/dot_general | solution.py:114
  146.2 2.8 fusion.93
  149.0 3.5 %fusion.96 = f32[1,2,512,128]{3,2,1,0:T(8,128)} fusion(f32[512,512,2]{1,0,2:T(8,128)} %get-tuple-element.223, f32[2,512]{1,0:T(2,128)S(1)} %bitcast.183, pred[512,512]{0,1:T(8,128)(4,1)S(1)} %broadcast_compare_fusion.2, f32[1,2,512,128]{3,2,1,0:T(8,128)} %get-tuple-element.239, f32[2,512]{1,0:T(2,128)S(1)} %get-tuple-element.224, pred[]{:T(512)S(6)} %compare.14, ...), kind=kOutput, calls=%fused_computation.8.clone.1 | convolution fusion | flops 137232384 | bytes 3547649 | tf_op jit(solution)/shard_map/cond/branch_1_fun/while/body/eval_jaxpr/kgqt,tkd->kgqd/dot_general | solution.py:114
  154.6 2.8 fusion.93
  157.4 3.5 %fusion.96 = f32[1,2,512,128]{3,2,1,0:T(8,128)} fusion(f32[512,512,2]{1,0,2:T(8,128)} %get-tuple-element.223, f32[2,512]{1,0:T(2,128)S(1)} %bitcast.183, pred[512,512]{0,1:T(8,128)(4,1)S(1)} %broadcast_compare_fusion.2, f32[1,2,512,128]{3,2,1,0:T(8,128)} %get-tuple-element.239, f32[2,512]{1,0:T(2,128)S(1)} %get-tuple-element.224, pred[]{:T(512)S(6)} %compare.14, ...), kind=kOutput, calls=%fused_computation.8.clone.1 | convolution fusion | flops 137232384 | bytes 3547649 | tf_op jit(solution)/shard_map/cond/branch_1_fun/while/body/eval_jaxpr/kgqt,tkd->kgqd/dot_general | solution.py:114
  165.2 3.4 %all-to-all-start = ((bf16[4,128,256]{2,1,0:T(8,128)(2,1)}), bf16[4,128,256]{2,1,0:T(8,128)(2,1)S(1)}, u32[]{:S(2)}, u32[]{:S(2)}) async-start(bf16[4,128,256]{2,1,0:T(8,128)(2,1)} %convert_element_type.116), calls=%async_computation | async-start | bytes 524288 | tf_op jit(solution)/shard_map/all_to_all | solution.py:132
  168.7 6.0 %all-to-all-done = bf16[4,128,256]{2,1,0:T(8,128)(2,1)S(1)} async-done(((bf16[4,128,256]{2,1,0:T(8,128)(2,1)}), bf16[4,128,256]{2,1,0:T(8,128)(2,1)S(1)}, u32[]{:S(2)}, u32[]{:S(2)}) %all-to-all-start) | async-done | bytes 262176 | tf_op jit(solution)/shard_map/all_to_all | solution.py:132
  175.3 3.1 fusion.80
  182.8 4.4 %scatter_custom_fusion = bf16[512,2048]{1,0:T(8,128)(2,1)} fusion(s32[256]{0:T(256)S(1)} %bitcast.190, bf16[256,2048]{1,0:T(8,128)(2,1)} %reshape.481, bf16[]{:T(256)} %constant.103.clone.1), kind=kCustom, calls=%fused_computation.51 | custom fusion | bytes 2097664 | tf_op jit(solution)/shard_map/scatter | solution.py:158
  187.3 51.5 %all_to_all.20 = bf16[32,16,2048]{2,1,0:T(8,128)(2,1)S(1)} all-to-all(bf16[32,16,2048]{2,1,0:T(8,128)(2,1)} %bitcast.181), channel_id=1, replica_groups=mesh['sp'=8,'tp'=4] {'sp','tp'}, dimensions={0} | all-to-all | bytes 4194304 | tf_op jit(solution)/shard_map/all_to_all | solution.py:160
  242.3 6.3 %convolution_convert_fusion = bf16[32,16,2048]{2,1,0:T(8,128)(2,1)} fusion(bf16[1,512,2048]{2,1,0:T(8,128)(2,1)S(1)} %copy-done, bf16[32,16,2048]{2,1,0:T(8,128)(2,1)} %copy-done.2, bf16[1,2048,512]{2,1,0:T(8,128)(2,1)} %param.36, f32[32,1,16,512]{3,2,0,1:T(8,128)} %fusion.29), kind=kOutput, calls=%fused_computation.35 | convolution fusion | flops 2150105088 | bytes 9437184 | tf_op jit(solution)/shard_map/sekf,efd->sekd/dot_general | solution.py:176
  248.6 3.7 %all-to-all-start.2 = ((bf16[32,16,2048]{2,1,0:T(8,128)(2,1)}), bf16[32,16,2048]{2,1,0:T(8,128)(2,1)}, u32[]{:S(2)}, u32[]{:S(2)}) async-start(bf16[32,16,2048]{2,1,0:T(8,128)(2,1)} %convolution_convert_fusion), calls=%async_computation.2 | async-start | bytes 4194304 | tf_op jit(solution)/shard_map/all_to_all | solution.py:177
  252.4 48.6 %all-to-all-done.2 = bf16[32,16,2048]{2,1,0:T(8,128)(2,1)} async-done(((bf16[32,16,2048]{2,1,0:T(8,128)(2,1)}), bf16[32,16,2048]{2,1,0:T(8,128)(2,1)}, u32[]{:S(2)}, u32[]{:S(2)}) %all-to-all-start.2) | async-done | bytes 2097184 | tf_op jit(solution)/shard_map/all_to_all | solution.py:177
  301.0 5.2 %gather_fusion = bf16[256,2048]{1,0:T(8,128)(2,1)} fusion(bf16[512,2048]{1,0:T(8,128)(2,1)} %bitcast.37, s32[1024]{0:T(1024)S(1)} %pad_clamp_fusion), kind=kCustom, calls=%fused_computation | custom fusion | bytes 2098176 | tf_op jit(solution)/shard_map/gather | solution.py:184
  306.2 3.4 %reshape.468 = f32[128,2,2048]{2,1,0:T(2,128)} reshape(bf16[256,2048]{1,0:T(8,128)(2,1)} %gather_fusion) | data formatting | bytes 3145728 | tf_op jit(solution)/shard_map/convert_element_type | solution.py:185
  309.6 4.8 %multiply_reduce_fusion = f32[128,2048]{1,0:T(8,128)S(1)} fusion(f32[128,2,2048]{2,1,0:T(2,128)} %reshape.468, f32[128,2]{1,0:T(8,128)S(1)} %copy.56), kind=kLoop, calls=%fused_computation.43 | loop fusion | flops 786432 | bytes 3146752 | tf_op jit(solution)/shard_map/reduce_sum | solution.py:186
  (153 shorter events, 39.5 us)
Async XLA Ops:
  6.5 235.8 %copy-start = (bf16[1,512,2048]{2,1,0:T(8,128)(2,1)S(1)}, bf16[1,512,2048]{2,1,0:T(8,128)(2,1)}, u32[]{:S(2)}) copy-start(bf16[1,512,2048]{2,1,0:T(8,128)(2,1)} %param.37) | copy-start | bytes 6291460
  6.5 4.1 %copy-start.10 = (s32[128,2]{0,1:T(2,128)S(1)}, s32[128,2]{0,1:T(2,128)}, u32[]{:S(2)}) copy-start(s32[128,2]{0,1:T(2,128)} %param.33) | copy-start | bytes 3076
  6.5 4.5 %copy-start.3 = (bf16[512,256]{1,0:T(8,128)(2,1)S(1)}, bf16[512,256]{1,0:T(8,128)(2,1)}, u32[]{:S(2)}) copy-start(bf16[512,256]{1,0:T(8,128)(2,1)} %param.22) | copy-start | bytes 786436
  6.5 4.7 %copy-start.6 = (s32[512]{0:T(512)S(1)}, s32[512]{0:T(512)}, u32[]{:S(2)}) copy-start(s32[512]{0:T(512)} %param.25) | copy-start | bytes 6148
  6.5 38.1 %copy-start.12 = (f32[128]{0:T(128)S(1)}, f32[128]{0:T(128)}, u32[]{:S(2)}) copy-start(f32[128]{0:T(128)} %param.26) | copy-start | bytes 1540
  6.5 45.6 %all-gather.4.cloned.1.call-start = ((), (), s32[]{:S(2)}) async-start(), calls=%async_computation.3 | async-start | bytes 1179648 | tf_op jit(solution)/shard_map/all_gather | solution.py:90
  9.9 83.7 %all-gather.6.cloned.1.call-start = ((), (), s32[]{:S(2)}) async-start(), calls=%async_computation.4 | async-start | bytes 1179648 | tf_op jit(solution)/shard_map/all_gather | solution.py:91
  99.2 3.4 %copy-start.1 = (f32[512,512,2]{1,0,2:T(8,128)S(1)}, f32[512,512,2]{1,0,2:T(8,128)}, u32[]{:S(2)}) copy-start(f32[512,512,2]{1,0,2:T(8,128)} %get-tuple-element.223) | copy-start | bytes 6291460 | tf_op jit(solution)/shard_map/cond/branch_1_fun/while
  106.8 3.5 %copy-start.1 = (f32[512,512,2]{1,0,2:T(8,128)S(1)}, f32[512,512,2]{1,0,2:T(8,128)}, u32[]{:S(2)}) copy-start(f32[512,512,2]{1,0,2:T(8,128)} %get-tuple-element.223) | copy-start | bytes 6291460 | tf_op jit(solution)/shard_map/cond/branch_1_fun/while
  115.3 3.5 %copy-start.1 = (f32[512,512,2]{1,0,2:T(8,128)S(1)}, f32[512,512,2]{1,0,2:T(8,128)}, u32[]{:S(2)}) copy-start(f32[512,512,2]{1,0,2:T(8,128)} %get-tuple-element.223) | copy-start | bytes 6291460 | tf_op jit(solution)/shard_map/cond/branch_1_fun/while
  123.7 3.5 %copy-start.1 = (f32[512,512,2]{1,0,2:T(8,128)S(1)}, f32[512,512,2]{1,0,2:T(8,128)}, u32[]{:S(2)}) copy-start(f32[512,512,2]{1,0,2:T(8,128)} %get-tuple-element.223) | copy-start | bytes 6291460 | tf_op jit(solution)/shard_map/cond/branch_1_fun/while
  132.1 3.5 %copy-start.1 = (f32[512,512,2]{1,0,2:T(8,128)S(1)}, f32[512,512,2]{1,0,2:T(8,128)}, u32[]{:S(2)}) copy-start(f32[512,512,2]{1,0,2:T(8,128)} %get-tuple-element.223) | copy-start | bytes 6291460 | tf_op jit(solution)/shard_map/cond/branch_1_fun/while
  140.6 3.5 %copy-start.1 = (f32[512,512,2]{1,0,2:T(8,128)S(1)}, f32[512,512,2]{1,0,2:T(8,128)}, u32[]{:S(2)}) copy-start(f32[512,512,2]{1,0,2:T(8,128)} %get-tuple-element.223) | copy-start | bytes 6291460 | tf_op jit(solution)/shard_map/cond/branch_1_fun/while
  149.0 3.5 %copy-start.1 = (f32[512,512,2]{1,0,2:T(8,128)S(1)}, f32[512,512,2]{1,0,2:T(8,128)}, u32[]{:S(2)}) copy-start(f32[512,512,2]{1,0,2:T(8,128)} %get-tuple-element.223) | copy-start | bytes 6291460 | tf_op jit(solution)/shard_map/cond/branch_1_fun/while
  157.4 3.5 %copy-start.1 = (f32[512,512,2]{1,0,2:T(8,128)S(1)}, f32[512,512,2]{1,0,2:T(8,128)}, u32[]{:S(2)}) copy-start(f32[512,512,2]{1,0,2:T(8,128)} %get-tuple-element.223) | copy-start | bytes 6291460 | tf_op jit(solution)/shard_map/cond/branch_1_fun/while
  162.8 12.2 %copy-start.9 = (f32[1024]{0:T(1024)S(1)}, f32[1024]{0:T(1024)}, u32[]{:S(2)}) copy-start(f32[1024]{0:T(1024)} %param.28) | copy-start | bytes 12292
  165.2 9.4 %all-to-all-start = ((bf16[4,128,256]{2,1,0:T(8,128)(2,1)}), bf16[4,128,256]{2,1,0:T(8,128)(2,1)S(1)}, u32[]{:S(2)}, u32[]{:S(2)}) async-start(bf16[4,128,256]{2,1,0:T(8,128)(2,1)} %convert_element_type.116), calls=%async_computation | async-start | bytes 524288 | tf_op jit(solution)/shard_map/all_to_all | solution.py:132
  175.2 3.4 %copy-start.4 = (f32[2048]{0:T(1024)S(1)}, f32[2048]{0:T(1024)}, u32[]{:S(2)}) copy-start(f32[2048]{0:T(1024)} %param.32) | copy-start | bytes 24580
  175.2 3.4 %copy-start.5 = (f32[2048]{0:T(1024)S(1)}, f32[2048]{0:T(1024)}, u32[]{:S(2)}) copy-start(f32[2048]{0:T(1024)} %param.31) | copy-start | bytes 24580
  187.3 52.8 %copy-start.13 = (bf16[1,2048,512]{2,1,0:T(8,128)(2,1)S(1)}, bf16[1,2048,512]{2,1,0:T(8,128)(2,1)}, u32[]{:S(2)}) copy-start(bf16[1,2048,512]{2,1,0:T(8,128)(2,1)} %param.35) | copy-start | bytes 6291460
  238.8 1.3 copy-start.2
  248.6 3.7 %copy-start.11 = (f32[128,2]{0,1:T(2,128)S(1)}, f32[128,2]{0,1:T(2,128)}, u32[]{:S(2)}) copy-start(f32[128,2]{0,1:T(2,128)} %param.34) | copy-start | bytes 3076
  248.6 52.4 %all-to-all-start.2 = ((bf16[32,16,2048]{2,1,0:T(8,128)(2,1)}), bf16[32,16,2048]{2,1,0:T(8,128)(2,1)}, u32[]{:S(2)}, u32[]{:S(2)}) async-start(bf16[32,16,2048]{2,1,0:T(8,128)(2,1)} %convolution_convert_fusion), calls=%async_computation.2 | async-start | bytes 4194304 | tf_op jit(solution)/shard_map/all_to_all | solution.py:177
  314.4 0.9 copy-start.7
  314.4 0.9 copy-start.8
Sparse Core Ops, SparseCore 0:
  10.0 42.1 all-gather.3
  54.3 39.2 all-gather.5
where the time goes:
time: 325 us; the launch traced here: 324 us
  waiting for transfers between devices  104 us (32%)
  blocking collectives  79.5 us (24%)
  matrix products  62.1 us (19%)
  other arithmetic  28.8 us (9%)
  local copies, waits for them, and re-layouts  25.6 us (8%)
  between operations  16.3 us (5%)
  starting transfers between devices  7.21 us (2%)
    all_to_all x1, blocking collectives, per_device(): lax.all_to_all(outbound.reshape(expert_total, capacity, model_width), ('s...  51.5 us
    all_to_all x1, waiting for transfers between devices, per_device(): lax.all_to_all(served.astype(jnp.bfloat16).reshape(arrived.shape), ('sp',...  48.6 us
    all_gather x1, waiting for transfers between devices, per_device(): value_part = lax.all_gather(value_heads, 'sp', axis=0, tiled=True)  41.4 us
    dot_general x8, matrix products, advance(): jnp.einsum('kgqt,tkd->kgqd', weights.astype(jnp.bfloat16), value_block, p...  28 us
    all_gather x1, blocking collectives, per_device(): doc_part = lax.all_gather(documents, 'sp', axis=0, tiled=True)  27.9 us
    dot_general x8, matrix products, advance(): jnp.einsum('qkgd,tkd->kgqt', query_rot, key_block, preferred_element_type...  22.4 us
    add x8, other arithmetic, advance(): new_total = running_total * rescale + jnp.sum(weights, axis=-1)  9.54 us
    all_gather x1, waiting for transfers between devices, per_device(): key_part = lax.all_gather(key_rot, 'sp', axis=0, tiled=True)  7.31 us
  transfers between devices with their start and end apart: 4, of which 4 were waited for; matrix products, arithmetic and copies ran while one was open for 1% of the time, Pallas kernels for 0%

commit v1 on v0

--- a/solution.py
+++ b/solution.py
@@ -3,6 +3,7 @@
 import jax.numpy as jnp
 from jax import lax
 from jax.sharding import PartitionSpec as P
+from jax.lax import all_to_all, axis_size
 
 HEAD = 128
 GRID = 64
@@ -88,7 +89,9 @@
         jnp.zeros((key_local, grouped, tok_rows, HEAD), jnp.float32),
     )
     key_part = lax.all_gather(key_rot, "sp", axis=0, tiled=True)
-    value_part = lax.all_gather(value_heads, "sp", axis=0, tiled=True)
+    value_part = jnp.concatenate(
+        all_to_all(jnp.stack([value_heads for _ in range(axis_size("sp"))]), "sp", 0, 0), axis=0
+    )
     doc_part = lax.all_gather(documents, "sp", axis=0, tiled=True)
     piece_rows = key_part.shape[0]
     block_rows = math.gcd(piece_rows, 512)

time: 325 us -> 304 us (0.935)
  waiting for transfers between devices: 104 us -> 54.6 us
  blocking collectives: 79.5 us -> 99.8 us
  starting transfers between devices: 7.21 us -> 14.6 us
    all_gather x1 -> x0, waiting for transfers between devices: 41.4 us -> none  [per_device(): value_part = lax.all_gather(value_heads, 'sp', axis=0, tiled=True)]
    all_gather x1, blocking collectives: 27.9 us -> 48.3 us  [per_device(): doc_part = lax.all_gather(documents, 'sp', axis=0, tiled=True)]
    all_to_all x0 -> x1, starting transfers between devices: none -> 7.44 us  [per_device(): all_to_all(jnp.stack([value_heads for _ in range(axis_size('sp'))]), 'sp'...]
    all_gather x1, waiting for transfers between devices: 7.31 us -> 0.02 us  [per_device(): key_part = lax.all_gather(key_rot, 'sp', axis=0, tiled=True)]
  transfers between devices with their start and end apart: 4 -> 4, of which waited for: 4 -> 2; matrix products, arithmetic and copies ran while one was open for 1% -> 2% of each run, Pallas kernels for 0% -> 0%
where the time goes in v1:
time: 304 us; the launch traced here: 303 us
  blocking collectives  99.8 us (33%)
  matrix products  62.1 us (20%)
  waiting for transfers between devices  54.6 us (18%)
  other arithmetic  28.8 us (9%)
  local copies, waits for them, and re-layouts  26.7 us (9%)
  between operations  16.3 us (5%)
  starting transfers between devices  14.6 us (5%)
    all_to_all x1, blocking collectives, per_device(): lax.all_to_all(outbound.reshape(expert_total, capacity, model_width), ('s...  51.5 us
    all_to_all x1, waiting for transfers between devices, per_device(): lax.all_to_all(served.astype(jnp.bfloat16).reshape(arrived.shape), ('sp',...  48.6 us
    all_gather x1, blocking collectives, per_device(): doc_part = lax.all_gather(documents, 'sp', axis=0, tiled=True)  48.3 us
    dot_general x8, matrix products, advance(): jnp.einsum('kgqt,tkd->kgqd', weights.astype(jnp.bfloat16), value_block, p...  28 us
    dot_general x8, matrix products, advance(): jnp.einsum('qkgd,tkd->kgqt', query_rot, key_block, preferred_element_type...  22.4 us
    add x8, other arithmetic, advance(): new_total = running_total * rescale + jnp.sum(weights, axis=-1)  9.54 us
    all_to_all x1, starting transfers between devices, per_device(): all_to_all(jnp.stack([value_heads for _ in range(axis_size('sp'))]), 'sp'...  7.44 us
    dot_general x1, matrix products, per_device(): jnp.einsum('sekf,efd->sekd', hidden, expert_down, preferred_element_type=...  6.27 us
  transfers between devices with their start and end apart: 4, of which 2 were waited for; matrix products, arithmetic and copies ran while one was open for 2% of the time, Pallas kernels for 0%

profile of v1, /device:TPU:0, one launch (start us, length us, event | category | flops | bytes accessed | tf_op | source)
XLA Modules:
  0.0 303.1 jit_solution(1333772610361120397)
XLA Ops:
  11.0 7.4 %all-to-all-start = ((bf16[8,512,128]{2,1,0:T(8,128)(2,1)}), bf16[8,512,128]{2,1,0:T(8,128)(2,1)}, u32[]{:S(2)}, u32[]{:S(2)}) async-start(bf16[8,512,128]{2,1,0:T(8,128)(2,1)} %stack.2), calls=%async_computation | async-start | bytes 2097152 | tf_op jit(solution)/shard_map/all_to_all | solution.py:93
  19.0 48.3 %all-gather = s32[8,1,512]{2,1,0:T(1,128)S(1)} all-gather(s32[1,1,512]{2,1,0:T(1,128)S(1)} %bitcast.186), channel_id=1, replica_groups=mesh['sp'=8,'tp'=4] {'sp'}, dimensions={0}, use_global_device_ids=true | all-gather | bytes 18432 | tf_op jit(solution)/shard_map/all_gather | solution.py:95
  73.1 69.2 %conditional.1 = (f32[1,2,512]{2,1,0:T(2,128)}, f32[1,2,512,128]{3,2,1,0:T(8,128)}) conditional(s32[]{:T(128)} %bitcast.4, () %tuple.17, (bf16[4096,128]{0,1:T(8,128)(2,1)}, bf16[8,512,128]{2,1,0:T(8,128)(2,1)}, s32[4096]{0:T(1024)S(1)}, s32[512]{0:T(512)S(1)}, bf16[512,1,2,128]{0,3,2,1:T(8,128)(2,1)S(1)}) %tuple.60), branch_computations={%region_2.3_spmd, %region_3.8_spmd} | conditional | flops 275912704 | bytes 20030728 | solution.py:130
  73.1 2.3 copy.48
  75.6 66.7 %while.14 = (s32[]{:T(128)}, f32[1,2,512]{2,1,0:T(2,128)S(1)}, f32[1,2,512]{2,1,0:T(2,128)}, f32[1,2,512,128]{3,2,1,0:T(8,128)}, s32[512]{0:T(512)S(1)}, /*index...) while((s32[]{:T(128)}, f32[1,2,512]{2,1,0:T(2,128)S(1)}, ...), condition=%wide.region_7.7_spmd.clone, body=%wide.region_4.6_spmd.clone.sunk | while | flops 275912704 | bytes 17376408 | solution.py:126
  75.9 2.8 fusion.93
  78.7 3.4 %fusion.96 = f32[1,2,512,128]{3,2,1,0:T(8,128)} fusion(f32[512,512,2]{1,0,2:T(8,128)} %get-tuple-element.223, f32[2,512]{1,0:T(2,128)S(1)} %bitcast.183, pred[512,512]{0,1:T(8,128)(4,1)S(1)} %broadcast_compare_fusion.2, f32[1,2,512,128]{3,2,1,0:T(8,128)} %get-tuple-element.239, f32[2,512]{1,0:T(2,128)S(1)} %get-tuple-element.224, pred[]{:T(512)S(6)} %compare.14, ...), kind=kOutput, calls=%fused_computation.8.clone.1 | convolution fusion | flops 137232384 | bytes 3547649 | tf_op jit(solution)/shard_map/cond/branch_1_fun/while/body/eval_jaxpr/kgqt,tkd->kgqd/dot_general | solution.py:117
  83.5 2.8 fusion.93
  86.4 3.5 %fusion.96 = f32[1,2,512,128]{3,2,1,0:T(8,128)} fusion(f32[512,512,2]{1,0,2:T(8,128)} %get-tuple-element.223, f32[2,512]{1,0:T(2,128)S(1)} %bitcast.183, pred[512,512]{0,1:T(8,128)(4,1)S(1)} %broadcast_compare_fusion.2, f32[1,2,512,128]{3,2,1,0:T(8,128)} %get-tuple-element.239, f32[2,512]{1,0:T(2,128)S(1)} %get-tuple-element.224, pred[]{:T(512)S(6)} %compare.14, ...), kind=kOutput, calls=%fused_computation.8.clone.1 | convolution fusion | flops 137232384 | bytes 3547649 | tf_op jit(solution)/shard_map/cond/branch_1_fun/while/body/eval_jaxpr/kgqt,tkd->kgqd/dot_general | solution.py:117
  92.0 2.8 fusion.93
  94.8 3.5 %fusion.96 = f32[1,2,512,128]{3,2,1,0:T(8,128)} fusion(f32[512,512,2]{1,0,2:T(8,128)} %get-tuple-element.223, f32[2,512]{1,0:T(2,128)S(1)} %bitcast.183, pred[512,512]{0,1:T(8,128)(4,1)S(1)} %broadcast_compare_fusion.2, f32[1,2,512,128]{3,2,1,0:T(8,128)} %get-tuple-element.239, f32[2,512]{1,0:T(2,128)S(1)} %get-tuple-element.224, pred[]{:T(512)S(6)} %compare.14, ...), kind=kOutput, calls=%fused_computation.8.clone.1 | convolution fusion | flops 137232384 | bytes 3547649 | tf_op jit(solution)/shard_map/cond/branch_1_fun/while/body/eval_jaxpr/kgqt,tkd->kgqd/dot_general | solution.py:117
  100.4 2.8 fusion.93
  103.2 3.5 %fusion.96 = f32[1,2,512,128]{3,2,1,0:T(8,128)} fusion(f32[512,512,2]{1,0,2:T(8,128)} %get-tuple-element.223, f32[2,512]{1,0:T(2,128)S(1)} %bitcast.183, pred[512,512]{0,1:T(8,128)(4,1)S(1)} %broadcast_compare_fusion.2, f32[1,2,512,128]{3,2,1,0:T(8,128)} %get-tuple-element.239, f32[2,512]{1,0:T(2,128)S(1)} %get-tuple-element.224, pred[]{:T(512)S(6)} %compare.14, ...), kind=kOutput, calls=%fused_computation.8.clone.1 | convolution fusion | flops 137232384 | bytes 3547649 | tf_op jit(solution)/shard_map/cond/branch_1_fun/while/body/eval_jaxpr/kgqt,tkd->kgqd/dot_general | solution.py:117
  108.8 2.8 fusion.93
  111.7 3.5 %fusion.96 = f32[1,2,512,128]{3,2,1,0:T(8,128)} fusion(f32[512,512,2]{1,0,2:T(8,128)} %get-tuple-element.223, f32[2,512]{1,0:T(2,128)S(1)} %bitcast.183, pred[512,512]{0,1:T(8,128)(4,1)S(1)} %broadcast_compare_fusion.2, f32[1,2,512,128]{3,2,1,0:T(8,128)} %get-tuple-element.239, f32[2,512]{1,0:T(2,128)S(1)} %get-tuple-element.224, pred[]{:T(512)S(6)} %compare.14, ...), kind=kOutput, calls=%fused_computation.8.clone.1 | convolution fusion | flops 137232384 | bytes 3547649 | tf_op jit(solution)/shard_map/cond/branch_1_fun/while/body/eval_jaxpr/kgqt,tkd->kgqd/dot_general | solution.py:117
  117.3 2.8 fusion.93
  120.1 3.5 %fusion.96 = f32[1,2,512,128]{3,2,1,0:T(8,128)} fusion(f32[512,512,2]{1,0,2:T(8,128)} %get-tuple-element.223, f32[2,512]{1,0:T(2,128)S(1)} %bitcast.183, pred[512,512]{0,1:T(8,128)(4,1)S(1)} %broadcast_compare_fusion.2, f32[1,2,512,128]{3,2,1,0:T(8,128)} %get-tuple-element.239, f32[2,512]{1,0:T(2,128)S(1)} %get-tuple-element.224, pred[]{:T(512)S(6)} %compare.14, ...), kind=kOutput, calls=%fused_computation.8.clone.1 | convolution fusion | flops 137232384 | bytes 3547649 | tf_op jit(solution)/shard_map/cond/branch_1_fun/while/body/eval_jaxpr/kgqt,tkd->kgqd/dot_general | solution.py:117
  125.7 2.8 fusion.93
  128.5 3.5 %fusion.96 = f32[1,2,512,128]{3,2,1,0:T(8,128)} fusion(f32[512,512,2]{1,0,2:T(8,128)} %get-tuple-element.223, f32[2,512]{1,0:T(2,128)S(1)} %bitcast.183, pred[512,512]{0,1:T(8,128)(4,1)S(1)} %broadcast_compare_fusion.2, f32[1,2,512,128]{3,2,1,0:T(8,128)} %get-tuple-element.239, f32[2,512]{1,0:T(2,128)S(1)} %get-tuple-element.224, pred[]{:T(512)S(6)} %compare.14, ...), kind=kOutput, calls=%fused_computation.8.clone.1 | convolution fusion | flops 137232384 | bytes 3547649 | tf_op jit(solution)/shard_map/cond/branch_1_fun/while/body/eval_jaxpr/kgqt,tkd->kgqd/dot_general | solution.py:117
  134.1 2.8 fusion.93
  137.0 3.5 %fusion.96 = f32[1,2,512,128]{3,2,1,0:T(8,128)} fusion(f32[512,512,2]{1,0,2:T(8,128)} %get-tuple-element.223, f32[2,512]{1,0:T(2,128)S(1)} %bitcast.183, pred[512,512]{0,1:T(8,128)(4,1)S(1)} %broadcast_compare_fusion.2, f32[1,2,512,128]{3,2,1,0:T(8,128)} %get-tuple-element.239, f32[2,512]{1,0:T(2,128)S(1)} %get-tuple-element.224, pred[]{:T(512)S(6)} %compare.14, ...), kind=kOutput, calls=%fused_computation.8.clone.1 | convolution fusion | flops 137232384 | bytes 3547649 | tf_op jit(solution)/shard_map/cond/branch_1_fun/while/body/eval_jaxpr/kgqt,tkd->kgqd/dot_general | solution.py:117
  144.8 3.4 %all-to-all-start.1 = ((bf16[4,128,256]{2,1,0:T(8,128)(2,1)}), bf16[4,128,256]{2,1,0:T(8,128)(2,1)S(1)}, u32[]{:S(2)}, u32[]{:S(2)}) async-start(bf16[4,128,256]{2,1,0:T(8,128)(2,1)} %convert_element_type.116), calls=%async_computation.1 | async-start | bytes 524288 | tf_op jit(solution)/shard_map/all_to_all | solution.py:135
  148.2 6.0 %all-to-all-done.1 = bf16[4,128,256]{2,1,0:T(8,128)(2,1)S(1)} async-done(((bf16[4,128,256]{2,1,0:T(8,128)(2,1)}), bf16[4,128,256]{2,1,0:T(8,128)(2,1)S(1)}, u32[]{:S(2)}, u32[]{:S(2)}) %all-to-all-start.1) | async-done | bytes 262176 | tf_op jit(solution)/shard_map/all_to_all | solution.py:135
  154.8 3.1 %fusion.80 = (f32[128]{0:T(128)S(1)}, f32[128,2048]{1,0:T(8,128)S(1)}) fusion(f32[128]{0:T(128)S(1)} %add_rsqrt_fusion.4, bf16[128,1024]{0,1:T(8,128)(2,1)S(1)} %fusion.51, bf16[1024,2048]{1,0:T(8,128)(2,1)} %param.29, bf16[128,2048]{1,0:T(8,128)(2,1)} %param.30), kind=kOutput, calls=%fused_computation.129 | convolution fusion | flops 538181504 | bytes 6030336 | tf_op jit(solution)/shard_map/dot_general | solution.py:139
  162.3 4.4 %scatter_custom_fusion = bf16[512,2048]{1,0:T(8,128)(2,1)} fusion(s32[256]{0:T(256)S(1)} %bitcast.190, bf16[256,2048]{1,0:T(8,128)(2,1)} %reshape.479, bf16[]{:T(256)} %constant.103.clone.1), kind=kCustom, calls=%fused_computation.51 | custom fusion | bytes 2097664 | tf_op jit(solution)/shard_map/scatter | solution.py:161
  166.8 51.5 %all_to_all.25 = bf16[32,16,2048]{2,1,0:T(8,128)(2,1)S(1)} all-to-all(bf16[32,16,2048]{2,1,0:T(8,128)(2,1)} %bitcast.181), channel_id=1, replica_groups=mesh['sp'=8,'tp'=4] {'sp','tp'}, dimensions={0} | all-to-all | bytes 4194304 | tf_op jit(solution)/shard_map/all_to_all | solution.py:163
  221.8 6.3 %convolution_convert_fusion = bf16[32,16,2048]{2,1,0:T(8,128)(2,1)} fusion(bf16[1,512,2048]{2,1,0:T(8,128)(2,1)S(1)} %copy-done, bf16[32,16,2048]{2,1,0:T(8,128)(2,1)} %copy-done.2, bf16[1,2048,512]{2,1,0:T(8,128)(2,1)} %param.36, f32[32,1,16,512]{3,2,0,1:T(8,128)} %fusion.29), kind=kOutput, calls=%fused_computation.35 | convolution fusion | flops 2150105088 | bytes 9437184 | tf_op jit(solution)/shard_map/sekf,efd->sekd/dot_general | solution.py:179
  228.1 3.7 %all-to-all-start.3 = ((bf16[32,16,2048]{2,1,0:T(8,128)(2,1)}), bf16[32,16,2048]{2,1,0:T(8,128)(2,1)}, u32[]{:S(2)}, u32[]{:S(2)}) async-start(bf16[32,16,2048]{2,1,0:T(8,128)(2,1)} %convolution_convert_fusion), calls=%async_computation.3 | async-start | bytes 4194304 | tf_op jit(solution)/shard_map/all_to_all | solution.py:180
  231.9 48.6 %all-to-all-done.3 = bf16[32,16,2048]{2,1,0:T(8,128)(2,1)} async-done(((bf16[32,16,2048]{2,1,0:T(8,128)(2,1)}), bf16[32,16,2048]{2,1,0:T(8,128)(2,1)}, u32[]{:S(2)}, u32[]{:S(2)}) %all-to-all-start.3) | async-done | bytes 2097184 | tf_op jit(solution)/shard_map/all_to_all | solution.py:180
  280.5 5.2 %gather_fusion = bf16[256,2048]{1,0:T(8,128)(2,1)} fusion(bf16[512,2048]{1,0:T(8,128)(2,1)} %bitcast.37, s32[1024]{0:T(1024)S(1)} %pad_clamp_fusion), kind=kCustom, calls=%fused_computation | custom fusion | bytes 2098176 | tf_op jit(solution)/shard_map/gather | solution.py:187
  285.7 3.4 %reshape.466 = f32[128,2,2048]{2,1,0:T(2,128)} reshape(bf16[256,2048]{1,0:T(8,128)(2,1)} %gather_fusion) | data formatting | bytes 3145728 | tf_op jit(solution)/shard_map/convert_element_type | solution.py:188
  289.1 4.8 %multiply_reduce_fusion = f32[128,2048]{1,0:T(8,128)S(1)} fusion(f32[128,2,2048]{2,1,0:T(2,128)} %reshape.466, f32[128,2]{1,0:T(8,128)S(1)} %copy.56), kind=kLoop, calls=%fused_computation.43 | loop fusion | flops 786432 | bytes 3146752 | tf_op jit(solution)/shard_map/reduce_sum | solution.py:189
  (155 shorter events, 37.7 us)
Async XLA Ops:
  6.5 215.3 %copy-start = (bf16[1,512,2048]{2,1,0:T(8,128)(2,1)S(1)}, bf16[1,512,2048]{2,1,0:T(8,128)(2,1)}, u32[]{:S(2)}) copy-start(bf16[1,512,2048]{2,1,0:T(8,128)(2,1)} %param.37) | copy-start | bytes 6291460
  6.5 3.3 %copy-start.6 = (bf16[512,128]{1,0:T(8,128)(2,1)S(1)}, bf16[512,128]{1,0:T(8,128)(2,1)}, u32[]{:S(2)}) copy-start(bf16[512,128]{1,0:T(8,128)(2,1)} %param.24) | copy-start | bytes 393220
  6.5 66.6 %all-gather.3.cloned.1.call-start = ((), (), s32[]{:S(2)}) async-start(), calls=%async_computation.4 | async-start | bytes 1179648 | tf_op jit(solution)/shard_map/all_gather | solution.py:91
  8.7 9.8 %copy-start.11 = (s32[128,2]{0,1:T(2,128)S(1)}, s32[128,2]{0,1:T(2,128)}, u32[]{:S(2)}) copy-start(s32[128,2]{0,1:T(2,128)} %param.33) | copy-start | bytes 3076
  8.7 10.2 %copy-start.3 = (bf16[512,256]{1,0:T(8,128)(2,1)S(1)}, bf16[512,256]{1,0:T(8,128)(2,1)}, u32[]{:S(2)}) copy-start(bf16[512,256]{1,0:T(8,128)(2,1)} %param.22) | copy-start | bytes 786436
  9.8 9.2 %copy-start.7 = (s32[512]{0:T(512)S(1)}, s32[512]{0:T(512)}, u32[]{:S(2)}) copy-start(s32[512]{0:T(512)} %param.25) | copy-start | bytes 6148
  11.0 61.8 %copy-start.13 = (f32[128]{0:T(128)S(1)}, f32[128]{0:T(128)}, u32[]{:S(2)}) copy-start(f32[128]{0:T(128)} %param.26) | copy-start | bytes 1540
  11.0 62.1 %all-to-all-start = ((bf16[8,512,128]{2,1,0:T(8,128)(2,1)}), bf16[8,512,128]{2,1,0:T(8,128)(2,1)}, u32[]{:S(2)}, u32[]{:S(2)}) async-start(bf16[8,512,128]{2,1,0:T(8,128)(2,1)} %stack.2), calls=%async_computation | async-start | bytes 2097152 | tf_op jit(solution)/shard_map/all_to_all | solution.py:93
  78.7 3.4 %copy-start.1 = (f32[512,512,2]{1,0,2:T(8,128)S(1)}, f32[512,512,2]{1,0,2:T(8,128)}, u32[]{:S(2)}) copy-start(f32[512,512,2]{1,0,2:T(8,128)} %get-tuple-element.223) | copy-start | bytes 6291460 | tf_op jit(solution)/shard_map/cond/branch_1_fun/while
  86.3 3.5 %copy-start.1 = (f32[512,512,2]{1,0,2:T(8,128)S(1)}, f32[512,512,2]{1,0,2:T(8,128)}, u32[]{:S(2)}) copy-start(f32[512,512,2]{1,0,2:T(8,128)} %get-tuple-element.223) | copy-start | bytes 6291460 | tf_op jit(solution)/shard_map/cond/branch_1_fun/while
  94.8 3.5 %copy-start.1 = (f32[512,512,2]{1,0,2:T(8,128)S(1)}, f32[512,512,2]{1,0,2:T(8,128)}, u32[]{:S(2)}) copy-start(f32[512,512,2]{1,0,2:T(8,128)} %get-tuple-element.223) | copy-start | bytes 6291460 | tf_op jit(solution)/shard_map/cond/branch_1_fun/while
  103.2 3.5 %copy-start.1 = (f32[512,512,2]{1,0,2:T(8,128)S(1)}, f32[512,512,2]{1,0,2:T(8,128)}, u32[]{:S(2)}) copy-start(f32[512,512,2]{1,0,2:T(8,128)} %get-tuple-element.223) | copy-start | bytes 6291460 | tf_op jit(solution)/shard_map/cond/branch_1_fun/while
  111.6 3.5 %copy-start.1 = (f32[512,512,2]{1,0,2:T(8,128)S(1)}, f32[512,512,2]{1,0,2:T(8,128)}, u32[]{:S(2)}) copy-start(f32[512,512,2]{1,0,2:T(8,128)} %get-tuple-element.223) | copy-start | bytes 6291460 | tf_op jit(solution)/shard_map/cond/branch_1_fun/while
  120.1 3.5 %copy-start.1 = (f32[512,512,2]{1,0,2:T(8,128)S(1)}, f32[512,512,2]{1,0,2:T(8,128)}, u32[]{:S(2)}) copy-start(f32[512,512,2]{1,0,2:T(8,128)} %get-tuple-element.223) | copy-start | bytes 6291460 | tf_op jit(solution)/shard_map/cond/branch_1_fun/while
  128.5 3.5 %copy-start.1 = (f32[512,512,2]{1,0,2:T(8,128)S(1)}, f32[512,512,2]{1,0,2:T(8,128)}, u32[]{:S(2)}) copy-start(f32[512,512,2]{1,0,2:T(8,128)} %get-tuple-element.223) | copy-start | bytes 6291460 | tf_op jit(solution)/shard_map/cond/branch_1_fun/while
  136.9 3.5 %copy-start.1 = (f32[512,512,2]{1,0,2:T(8,128)S(1)}, f32[512,512,2]{1,0,2:T(8,128)}, u32[]{:S(2)}) copy-start(f32[512,512,2]{1,0,2:T(8,128)} %get-tuple-element.223) | copy-start | bytes 6291460 | tf_op jit(solution)/shard_map/cond/branch_1_fun/while
  142.3 12.2 %copy-start.10 = (f32[1024]{0:T(1024)S(1)}, f32[1024]{0:T(1024)}, u32[]{:S(2)}) copy-start(f32[1024]{0:T(1024)} %param.28) | copy-start | bytes 12292
  144.8 9.4 %all-to-all-start.1 = ((bf16[4,128,256]{2,1,0:T(8,128)(2,1)}), bf16[4,128,256]{2,1,0:T(8,128)(2,1)S(1)}, u32[]{:S(2)}, u32[]{:S(2)}) async-start(bf16[4,128,256]{2,1,0:T(8,128)(2,1)} %convert_element_type.116), calls=%async_computation.1 | async-start | bytes 524288 | tf_op jit(solution)/shard_map/all_to_all | solution.py:135
  154.7 3.4 %copy-start.4 = (f32[2048]{0:T(1024)S(1)}, f32[2048]{0:T(1024)}, u32[]{:S(2)}) copy-start(f32[2048]{0:T(1024)} %param.32) | copy-start | bytes 24580
  154.8 3.4 %copy-start.5 = (f32[2048]{0:T(1024)S(1)}, f32[2048]{0:T(1024)}, u32[]{:S(2)}) copy-start(f32[2048]{0:T(1024)} %param.31) | copy-start | bytes 24580
  166.8 52.8 %copy-start.14 = (bf16[1,2048,512]{2,1,0:T(8,128)(2,1)S(1)}, bf16[1,2048,512]{2,1,0:T(8,128)(2,1)}, u32[]{:S(2)}) copy-start(bf16[1,2048,512]{2,1,0:T(8,128)(2,1)} %param.35) | copy-start | bytes 6291460
  218.3 1.3 copy-start.2
  228.1 3.7 %copy-start.12 = (f32[128,2]{0,1:T(2,128)S(1)}, f32[128,2]{0,1:T(2,128)}, u32[]{:S(2)}) copy-start(f32[128,2]{0,1:T(2,128)} %param.34) | copy-start | bytes 3076
  228.1 52.4 %all-to-all-start.3 = ((bf16[32,16,2048]{2,1,0:T(8,128)(2,1)}), bf16[32,16,2048]{2,1,0:T(8,128)(2,1)}, u32[]{:S(2)}, u32[]{:S(2)}) async-start(bf16[32,16,2048]{2,1,0:T(8,128)(2,1)} %convolution_convert_fusion), calls=%async_computation.3 | async-start | bytes 4194304 | tf_op jit(solution)/shard_map/all_to_all | solution.py:180
  293.9 0.9 copy-start.8
  293.9 0.9 copy-start.9
Sparse Core Ops, SparseCore 0:
  10.0 52.4 all-gather.2
